TPU v7x, 32 devices: a whole 2x2x4 slice. The times are simulated.
32 devices in a mesh: sp: 4 (over z), dp: 8 (over y, x, core).
Axes of the slice: x: 2, y: 2, z: 4, core: 2. Of those that a mesh axis runs over, the one named last changes fastest.
Arguments:
- queries: bfloat16 [8, 512, 1024], P('dp', 'sp'), may hold values from -6 to 6
- key_rows: bfloat16 [8, 512, 1024], P('dp', 'sp'), may hold values from -6 to 6
- values: bfloat16 [8, 512, 2048], P('dp', 'sp'), may hold values from -6 to 6
- out_gate: bfloat16 [8, 512, 2048], P('dp', 'sp'), may hold values from -6 to 6
- input_gate: bfloat16 [8, 4, 512], P('dp', None, 'sp'), may hold values from -6 to 205
- forget_gate: bfloat16 [8, 4, 512], P('dp', None, 'sp'), may hold values from 0.5 to 13
- out_weight: bfloat16 [2048, 2048], P(None, 'dp'), may hold values from -0.125 to 0.125
Outputs:
- layer_out: bfloat16 [8, 512, 2048], P('dp', 'sp')
All inputs are finite; a program needn't handle non-finite values.
Results may differ from a plain program's by a relative error of at most 0.0057.
Values may be sent and summed in bfloat16 or wider, within the bound.
A program may use at most 64 MiB of HBM per device.

v0:
```python
import jax
import jax.numpy as jnp
from jax import lax
from jax.sharding import PartitionSpec as P

BLOCK = 128


def memory_cell(query_rows, key_in, value_rows, input_log, forget_log):
    block_count = query_rows.shape[0] // BLOCK
    key_width = query_rows.shape[1]
    value_width = value_rows.shape[1]
    key_scale = key_width ** (-0.5)
    causal = lax.broadcasted_iota(jnp.int32, (BLOCK, BLOCK), 0) >= lax.broadcasted_iota(
        jnp.int32, (BLOCK, BLOCK), 1
    )
    highest = lax.Precision.HIGHEST

    def block_step(state_in, inputs):
        memory, normer, stabil = state_in
        query_part, key_part, value_part, gain_part, decay_part = inputs
        query_part = query_part.astype(jnp.float32)
        key_part = key_part.astype(jnp.float32) * key_scale
        value_part = value_part.astype(jnp.float32)
        running = jnp.cumsum(decay_part)
        log_weight = running[:, None] - running[None, :] + gain_part[None, :]
        log_weight = jnp.where(causal, log_weight, -jnp.inf)
        carried_log = running + stabil
        row_top = jnp.maximum(carried_log, jnp.max(log_weight, axis=1))
        scores = jnp.dot(query_part, key_part.T, precision=highest) * jnp.exp(
            log_weight - row_top[:, None]
        )
        carried = jnp.exp(carried_log - row_top)
        numerator = jnp.dot(scores, value_part, precision=highest) + carried[:, None] * jnp.dot(
            query_part, memory, precision=highest
        )
        denominator = jnp.sum(scores, axis=1) + carried * jnp.dot(
            query_part, normer, precision=highest
        )
        output = numerator / jnp.maximum(jnp.abs(denominator), 1.0)[:, None]
        block_end = running[-1]
        weight_log = block_end - running + gain_part
        new_top = jnp.maximum(block_end + stabil, jnp.max(weight_log))
        weights = jnp.exp(weight_log - new_top)
        retain = jnp.exp(block_end + stabil - new_top)
        memory = retain * memory + jnp.dot(
            (key_part * weights[:, None]).T, value_part, precision=highest
        )
        normer = retain * normer + jnp.dot(weights, key_part, precision=highest)
        return ((memory, normer, new_top), output)

    start_state = (
        jnp.zeros((key_width, value_width), jnp.float32),
        jnp.zeros((key_width,), jnp.float32),
        jnp.zeros((), jnp.float32),
    )
    blocks = tuple(
        (
            source.reshape((block_count, BLOCK) + source.shape[1:])
            for source in (query_rows, key_in, value_rows, input_log, forget_log)
        )
    )
    _, outputs = lax.scan(block_step, start_state, blocks)
    return outputs.reshape(block_count * BLOCK, value_width)


def body(queries, key_rows, values, out_gate, input_gate, forget_gate, out_weight):
    group_count = lax.axis_size("sp")
    token_count = queries.shape[1]
    head_count = input_gate.shape[1]
    copies = group_count // head_count
    head_key = queries.shape[2] // head_count
    slice_width = values.shape[2] // group_count

    def spread(source):
        widened = jnp.broadcast_to(
            source[0].reshape(token_count, head_count, 1, head_key),
            (token_count, head_count, copies, head_key),
        )
        return widened.reshape(token_count, group_count, head_key)

    def spread_gate(source):
        return jnp.repeat(source[0].T, copies, axis=1)

    query_all, key_all = (
        lax.all_to_all(spread(queries), "sp", split_axis=1, concat_axis=0, tiled=True),
        lax.all_to_all(spread(key_rows), "sp", split_axis=1, concat_axis=0, tiled=True),
    )
    value_all, input_all, forget_all = (
        lax.all_to_all(
            values[0].reshape(token_count, group_count, slice_width),
            "sp",
            split_axis=1,
            concat_axis=0,
            tiled=True,
        ),
        lax.all_to_all(spread_gate(input_gate), "sp", split_axis=1, concat_axis=0, tiled=True),
        lax.all_to_all(spread_gate(forget_gate), "sp", split_axis=1, concat_axis=0, tiled=True),
    )
    output = memory_cell(
        query_all[:, 0],
        key_all[:, 0],
        value_all[:, 0],
        input_all[:, 0].astype(jnp.float32),
        jax.nn.log_sigmoid(forget_all[:, 0].astype(jnp.float32)),
    )
    hidden = output.astype(jnp.bfloat16)
    token_rows = lax.all_to_all(hidden, "sp", split_axis=0, concat_axis=1, tiled=True)
    gated_rows = (
        token_rows.astype(jnp.float32) * jax.nn.sigmoid(out_gate[0].astype(jnp.float32))
    ).astype(jnp.bfloat16)
    projected = jnp.dot(
        gated_rows,
        lax.all_gather(out_weight, "dp", axis=1, tiled=True),
        preferred_element_type=jnp.float32,
    )
    return projected.astype(jnp.bfloat16)[None]


def solution(mesh):
    return jax.shard_map(
        body,
        mesh=mesh,
        in_specs=(
            P("dp", "sp", None),
            P("dp", "sp", None),
            P("dp", "sp", None),
            P("dp", "sp", None),
            P("dp", None, "sp"),
            P("dp", None, "sp"),
            P(None, "dp"),
        ),
        out_specs=P("dp", "sp", None),
        check_vma=False,
    )
```

profile of v0, /device:TPU:0, one launch (start us, length us, event | category | flops | bytes accessed | tf_op | source)
XLA Modules:
  0.0 121.6 jit_solution(9997319030571958665)
XLA Ops:
  6.5 0.7 all-gather.2.cloned.1.call-update
  7.3 1.3 %copy.28 = bf16[128,4,1]{0,2,1:T(2,128)(2,1)} copy(bf16[128,4,1]{0,1,2:T(4,128)(2,1)} %bitcast.152) | data formatting | bytes 2048 | tf_op jit(solution)/shard_map/all_to_all | solution.py:98
  8.5 6.3 %all-to-all-start = ((bf16[128,4,1]{0,2,1:T(2,128)(2,1)}), bf16[128,4,1]{0,2,1:T(2,128)(2,1)S(1)}, u32[]{:S(2)}, u32[]{:S(2)}) async-start(bf16[128,4,1]{0,2,1:T(2,128)(2,1)} %copy.28), calls=%async_computation | async-start | bytes 4096 | tf_op jit(solution)/shard_map/all_to_all | solution.py:98
  14.9 1.3 %copy.29 = bf16[128,4,1]{0,2,1:T(2,128)(2,1)} copy(bf16[128,4,1]{0,1,2:T(4,128)(2,1)} %bitcast.153) | data formatting | bytes 2048 | tf_op jit(solution)/shard_map/all_to_all | solution.py:97
  16.1 4.2 %all-to-all-done = bf16[128,4,1]{0,2,1:T(2,128)(2,1)S(1)} async-done(((bf16[128,4,1]{0,2,1:T(2,128)(2,1)}), bf16[128,4,1]{0,2,1:T(2,128)(2,1)S(1)}, u32[]{:S(2)}, u32[]{:S(2)}) %all-to-all-start) | async-done | bytes 1056 | tf_op jit(solution)/shard_map/all_to_all | solution.py:98
  20.4 3.2 %all-to-all-start.1 = ((bf16[128,4,1]{0,2,1:T(2,128)(2,1)}), bf16[128,4,1]{0,2,1:T(2,128)(2,1)S(1)}, u32[]{:S(2)}, u32[]{:S(2)}) async-start(bf16[128,4,1]{0,2,1:T(2,128)(2,1)} %copy.29), calls=%async_computation.1 | async-start | bytes 4096 | tf_op jit(solution)/shard_map/all_to_all | solution.py:97
  23.6 1.8 %copy.30 = bf16[1,128,1024]{1,2,0:T(8,128)(2,1)} copy(bf16[1,128,1024]{2,1,0:T(8,128)(2,1)} %param.10) | data formatting | bytes 524288 | tf_op args[1]
  25.4 3.6 %all-to-all-done.1 = bf16[128,4,1]{0,2,1:T(2,128)(2,1)S(1)} async-done(((bf16[128,4,1]{0,2,1:T(2,128)(2,1)}), bf16[128,4,1]{0,2,1:T(2,128)(2,1)S(1)}, u32[]{:S(2)}, u32[]{:S(2)}) %all-to-all-start.1) | async-done | bytes 1056 | tf_op jit(solution)/shard_map/all_to_all | solution.py:97
  29.0 3.4 %all-to-all-start.2 = ((bf16[128,4,256]{0,2,1:T(8,128)(2,1)}), bf16[128,4,256]{0,2,1:T(8,128)(2,1)S(1)}, u32[]{:S(2)}, u32[]{:S(2)}) async-start(bf16[128,4,256]{0,2,1:T(8,128)(2,1)} %bitcast.11), calls=%async_computation.2 | async-start | bytes 524288 | tf_op jit(solution)/shard_map/all_to_all | solution.py:87
  32.4 1.8 %copy.32 = bf16[1,128,1024]{1,2,0:T(8,128)(2,1)} copy(bf16[1,128,1024]{2,1,0:T(8,128)(2,1)} %param.9) | data formatting | bytes 524288 | tf_op args[0]
  34.2 4.9 %all-to-all-done.2 = bf16[128,4,256]{0,2,1:T(8,128)(2,1)S(1)} async-done(((bf16[128,4,256]{0,2,1:T(8,128)(2,1)}), bf16[128,4,256]{0,2,1:T(8,128)(2,1)S(1)}, u32[]{:S(2)}, u32[]{:S(2)}) %all-to-all-start.2) | async-done | bytes 262176 | tf_op jit(solution)/shard_map/all_to_all | solution.py:87
  39.1 3.4 %all-to-all-start.4 = ((bf16[128,4,256]{0,2,1:T(8,128)(2,1)}), bf16[128,4,256]{0,2,1:T(8,128)(2,1)S(1)}, u32[]{:S(2)}, u32[]{:S(2)}) async-start(bf16[128,4,256]{0,2,1:T(8,128)(2,1)} %bitcast.19), calls=%async_computation.4 | async-start | bytes 524288 | tf_op jit(solution)/shard_map/all_to_all | solution.py:86
  42.6 2.1 %copy.31 = bf16[1,128,2048]{1,2,0:T(8,128)(2,1)} copy(bf16[1,128,2048]{2,1,0:T(8,128)(2,1)} %param.11) | data formatting | bytes 1048576 | tf_op args[2]
  44.7 4.7 %all-to-all-done.4 = bf16[128,4,256]{0,2,1:T(8,128)(2,1)S(1)} async-done(((bf16[128,4,256]{0,2,1:T(8,128)(2,1)}), bf16[128,4,256]{0,2,1:T(8,128)(2,1)S(1)}, u32[]{:S(2)}, u32[]{:S(2)}) %all-to-all-start.4) | async-done | bytes 262176 | tf_op jit(solution)/shard_map/all_to_all | solution.py:86
  49.4 3.5 %all-to-all-start.3 = ((bf16[128,4,512]{0,2,1:T(8,128)(2,1)}), bf16[128,4,512]{0,2,1:T(8,128)(2,1)S(1)}, u32[]{:S(2)}, u32[]{:S(2)}) async-start(bf16[128,4,512]{0,2,1:T(8,128)(2,1)} %bitcast.15), calls=%async_computation.3 | async-start | bytes 1048576 | tf_op jit(solution)/shard_map/all_to_all | solution.py:90
  52.9 10.2 %all-to-all-done.3 = bf16[128,4,512]{0,2,1:T(8,128)(2,1)S(1)} async-done(((bf16[128,4,512]{0,2,1:T(8,128)(2,1)}), bf16[128,4,512]{0,2,1:T(8,128)(2,1)S(1)}, u32[]{:S(2)}, u32[]{:S(2)}) %all-to-all-start.3) | async-done | bytes 524320 | tf_op jit(solution)/shard_map/all_to_all | solution.py:90
  63.1 32.2 %while.17 = (s32[]{:T(128)}, f32[256,512]{1,0:T(8,128)S(1)}, f32[256]{0:T(256)S(1)}, f32[]{:T(128)}, bf16[4,128,512]{1,2,0:T(8,128)(2,1)}, /*index=5*/f32[4,128]...) while((s32[]{:T(128)}, f32[256,512]{1,0:T(8,128)S(1)}, ...), condition=%wide.region_5.6_spmd.clone, body=%wide.region_0.5_spmd.clone.sunk | while | flops 555633152 | bytes 3825425 | solution.py:63
  63.2 0.2 broadcast_in_dim.43
  63.4 0.6 slice.7
  64.0 0.8 subtract_reduce_fusion.2
  64.7 1.3 %fusion.87 = (f32[]{:T(128)}, f32[128]{0:T(128)S(1)}) fusion(f32[128]{0:T(128)S(1)} %get-tuple-element.231, f32[]{:T(128)} %bitcast.142, f32[4,128]{1,0:T(4,128)S(1)} %get-tuple-element.274, s32[]{:T(128)} %get-tuple-element.255), kind=kLoop, calls=%fused_computation.63.clone.1 | loop fusion | flops 383 | bytes 1548 | tf_op jit(solution)/shard_map/while/body/eval_jaxpr/reduce_max | solution.py:43
  67.5 0.2 fusion.89
  67.9 0.7 subtract_exponential_fusion.2
  68.6 0.2 fusion.90
  69.0 0.3 fusion.91
  69.3 0.4 fusion.93
  69.8 0.7 constant_dynamic-update-slice_fusion.2
  70.5 0.6 convolution_add_fusion.2
  71.4 0.6 slice.7
  72.0 0.8 subtract_reduce_fusion.2
  72.8 1.3 %fusion.87 = (f32[]{:T(128)}, f32[128]{0:T(128)S(1)}) fusion(f32[128]{0:T(128)S(1)} %get-tuple-element.231, f32[]{:T(128)} %bitcast.142, f32[4,128]{1,0:T(4,128)S(1)} %get-tuple-element.274, s32[]{:T(128)} %get-tuple-element.255), kind=kLoop, calls=%fused_computation.63.clone.1 | loop fusion | flops 383 | bytes 1548 | tf_op jit(solution)/shard_map/while/body/eval_jaxpr/reduce_max | solution.py:43
  75.6 0.2 fusion.89
  76.0 0.7 subtract_exponential_fusion.2
  76.6 0.2 fusion.90
  77.0 0.3 fusion.91
  77.4 0.4 fusion.93
  77.9 0.7 constant_dynamic-update-slice_fusion.2
  78.5 0.6 convolution_add_fusion.2
  79.3 0.2 broadcast_in_dim.43
  79.5 0.6 slice.7
  80.0 0.8 subtract_reduce_fusion.2
  80.8 1.3 %fusion.87 = (f32[]{:T(128)}, f32[128]{0:T(128)S(1)}) fusion(f32[128]{0:T(128)S(1)} %get-tuple-element.231, f32[]{:T(128)} %bitcast.142, f32[4,128]{1,0:T(4,128)S(1)} %get-tuple-element.274, s32[]{:T(128)} %get-tuple-element.255), kind=kLoop, calls=%fused_computation.63.clone.1 | loop fusion | flops 383 | bytes 1548 | tf_op jit(solution)/shard_map/while/body/eval_jaxpr/reduce_max | solution.py:43
  83.6 0.2 fusion.89
  84.0 0.7 subtract_exponential_fusion.2
  84.7 0.2 fusion.90
  85.1 0.3 fusion.91
  85.4 0.4 fusion.93
  85.9 0.7 constant_dynamic-update-slice_fusion.2
  86.6 0.6 convolution_add_fusion.2
  87.5 0.6 slice.7
  88.1 0.8 subtract_reduce_fusion.2
  88.9 1.3 %fusion.87 = (f32[]{:T(128)}, f32[128]{0:T(128)S(1)}) fusion(f32[128]{0:T(128)S(1)} %get-tuple-element.231, f32[]{:T(128)} %bitcast.142, f32[4,128]{1,0:T(4,128)S(1)} %get-tuple-element.274, s32[]{:T(128)} %get-tuple-element.255), kind=kLoop, calls=%fused_computation.63.clone.1 | loop fusion | flops 383 | bytes 1548 | tf_op jit(solution)/shard_map/while/body/eval_jaxpr/reduce_max | solution.py:43
  91.7 0.2 fusion.89
  92.0 0.7 subtract_exponential_fusion.2
  92.7 0.2 fusion.90
  93.1 0.3 fusion.91
  93.4 0.4 fusion.93
  94.0 0.7 constant_dynamic-update-slice_fusion.2
  94.6 0.6 convolution_add_fusion.2
  95.2 3.5 %all-to-all-start.5 = ((bf16[4,128,512]{1,2,0:T(8,128)(2,1)}), bf16[4,128,512]{1,2,0:T(8,128)(2,1)S(1)}, u32[]{:S(2)}, u32[]{:S(2)}) async-start(bf16[4,128,512]{1,2,0:T(8,128)(2,1)} %get-tuple-element.62), calls=%async_computation.5 | async-start | bytes 1048576 | tf_op jit(solution)/shard_map/all_to_all | solution.py:108
  98.7 0.3 copy.37
  99.0 10.0 %all-to-all-done.5 = bf16[4,128,512]{1,2,0:T(8,128)(2,1)S(1)} async-done(((bf16[4,128,512]{1,2,0:T(8,128)(2,1)}), bf16[4,128,512]{1,2,0:T(8,128)(2,1)S(1)}, u32[]{:S(2)}, u32[]{:S(2)}) %all-to-all-start.5) | async-done | bytes 524320 | tf_op jit(solution)/shard_map/all_to_all | solution.py:108
  109.0 0.3 fusion.50
  109.3 5.5 %fusion.49 = bf16[1,128,2048]{2,1,0:T(8,128)(2,1)} fusion(bf16[128,2048]{0,1:T(8,128)(2,1)S(1)} %fusion.50, bf16[2048,2048]{1,0:T(8,128)(2,1)} %all-gather.2.cloned.1.call-done), kind=kOutput, calls=%fused_computation.65 | convolution fusion | flops 1074003968 | bytes 9437184 | tf_op jit(solution)/shard_map/dot_general | solution.py:112
  (44 shorter events, 2.9 us)
Async XLA Ops:
  6.5 102.8 %all-gather.2.cloned.1.call-start = ((), (), s32[]{:S(2)}) async-start(), calls=%async_computation.6 | async-start | bytes 9437184 | tf_op jit(solution)/shard_map/all_gather | solution.py:114
  8.5 11.8 %all-to-all-start = ((bf16[128,4,1]{0,2,1:T(2,128)(2,1)}), bf16[128,4,1]{0,2,1:T(2,128)(2,1)S(1)}, u32[]{:S(2)}, u32[]{:S(2)}) async-start(bf16[128,4,1]{0,2,1:T(2,128)(2,1)} %copy.28), calls=%async_computation | async-start | bytes 4096 | tf_op jit(solution)/shard_map/all_to_all | solution.py:98
  20.4 8.6 %all-to-all-start.1 = ((bf16[128,4,1]{0,2,1:T(2,128)(2,1)}), bf16[128,4,1]{0,2,1:T(2,128)(2,1)S(1)}, u32[]{:S(2)}, u32[]{:S(2)}) async-start(bf16[128,4,1]{0,2,1:T(2,128)(2,1)} %copy.29), calls=%async_computation.1 | async-start | bytes 4096 | tf_op jit(solution)/shard_map/all_to_all | solution.py:97
  29.0 10.2 %all-to-all-start.2 = ((bf16[128,4,256]{0,2,1:T(8,128)(2,1)}), bf16[128,4,256]{0,2,1:T(8,128)(2,1)S(1)}, u32[]{:S(2)}, u32[]{:S(2)}) async-start(bf16[128,4,256]{0,2,1:T(8,128)(2,1)} %bitcast.11), calls=%async_computation.2 | async-start | bytes 524288 | tf_op jit(solution)/shard_map/all_to_all | solution.py:87
  39.1 10.2 %all-to-all-start.4 = ((bf16[128,4,256]{0,2,1:T(8,128)(2,1)}), bf16[128,4,256]{0,2,1:T(8,128)(2,1)S(1)}, u32[]{:S(2)}, u32[]{:S(2)}) async-start(bf16[128,4,256]{0,2,1:T(8,128)(2,1)} %bitcast.19), calls=%async_computation.4 | async-start | bytes 524288 | tf_op jit(solution)/shard_map/all_to_all | solution.py:86
  49.4 13.7 %all-to-all-start.3 = ((bf16[128,4,512]{0,2,1:T(8,128)(2,1)}), bf16[128,4,512]{0,2,1:T(8,128)(2,1)S(1)}, u32[]{:S(2)}, u32[]{:S(2)}) async-start(bf16[128,4,512]{0,2,1:T(8,128)(2,1)} %bitcast.15), calls=%async_computation.3 | async-start | bytes 1048576 | tf_op jit(solution)/shard_map/all_to_all | solution.py:90
  63.1 35.7 %copy-start = (bf16[1,128,2048]{2,1,0:T(8,128)(2,1)S(1)}, bf16[1,128,2048]{2,1,0:T(8,128)(2,1)}, u32[]{:S(2)}) copy-start(bf16[1,128,2048]{2,1,0:T(8,128)(2,1)} %param.12) | copy-start | bytes 1572868
  95.2 13.7 %all-to-all-start.5 = ((bf16[4,128,512]{1,2,0:T(8,128)(2,1)}), bf16[4,128,512]{1,2,0:T(8,128)(2,1)S(1)}, u32[]{:S(2)}, u32[]{:S(2)}) async-start(bf16[4,128,512]{1,2,0:T(8,128)(2,1)} %get-tuple-element.62), calls=%async_computation.5 | async-start | bytes 1048576 | tf_op jit(solution)/shard_map/all_to_all | solution.py:108
Sparse Core Ops, SparseCore 0:
  9.2 58.5 all-gather.1
where the time goes:
time: 122 us
  waiting for transfers between devices  38.3 us (31%)
  starting transfers between devices  23.4 us (19%)
  local copies, waits for them, and re-layouts  15 us (12%)
  between operations  13.5 us (11%)
  matrix products  12.9 us (11%)
  other arithmetic  12.7 us (10%)
  loops' own time  5.83 us (5%)
    all_to_all x1, waiting for transfers between devices, body(): lax.all_to_all(values[0].reshape(token_count, group_count, slice_width),...  10.2 us
    all_to_all x1, waiting for transfers between devices, body(): lax.all_to_all(hidden, 'sp', split_axis=0, concat_axis=1, tiled=True)  9.97 us
    all_to_all x1, starting transfers between devices, body(): lax.all_to_all(spread_gate(forget_gate), 'sp', split_axis=1, concat_axis=...  6.35 us
    unnamed x6, local copies, waits for them, and re-layouts  6 us
    another operation x1, loops' own time, memory_cell(): _, outputs = lax.scan(block_step, start_state, blocks)  5.83 us
    dot_general x1, matrix products, body(): jnp.dot(gated_rows, lax.all_gather(out_weight, 'dp', axis=1, tiled=True),...  5.46 us
    reduce_max x4, other arithmetic, block_step(): new_top = jnp.maximum(block_end + stabil, jnp.max(weight_log))  5.38 us
    all_to_all x1, waiting for transfers between devices, body(): lax.all_to_all(spread(key_rows), 'sp', split_axis=1, concat_axis=0, tiled...  4.92 us
  transfers between devices with their start and end apart: 7, of which 6 were waited for; matrix products, arithmetic and copies ran while one was open for 29% of the time, Pallas kernels for 0%

commit v1 on v0

v1 whole, which is shorter than its diff:
```python
import functools

import jax
import jax.numpy as jnp
from jax import lax
from jax.experimental import pallas as pl
from jax.experimental.pallas import tpu as pltpu
from jax.sharding import PartitionSpec as P

F32 = jnp.float32
BF16 = jnp.bfloat16
MESH = pl.DeviceIdType.MESH
PIECES = 8
HIGHEST = lax.Precision.HIGHEST


def flip(index, bit):
    return index + bit * (1 - 2 * ((index // bit) % 2))


def split_dot(left, right):
    if right.dtype == BF16:
        return jnp.dot(left, right, preferred_element_type=F32)
    high = right.astype(BF16)
    low = (right - high.astype(F32)).astype(BF16)
    return jnp.dot(left, high, preferred_element_type=F32) + jnp.dot(
        left, low, preferred_element_type=F32
    )


def kernel(
    n_sp, n_dp, heads, gather,
    q_ref, k_ref, v_ref, gate_ref, in_ref, forget_ref, w_ref, o_ref,
    rows_ref, cols_ref, kw_ref, nloc_ref, kv_ref, num_ref, gated_ref,
    aux_in, aux_out, state_in, state_out, aux_sem, state_send, state_recv,
    *w_scratch,
):
    z = lax.axis_index("sp")
    d = lax.axis_index("dp")
    tokens = q_ref.shape[1]
    dk = q_ref.shape[2] // heads
    dv = v_ref.shape[2] // heads
    scale = dk ** (-0.5)
    total = state_in.shape[0]
    per_head = total // heads
    wide = state_in.shape[2]
    last = n_sp - 1

    barrier = pltpu.get_barrier_semaphore()
    count = 0
    if gather:
        for bit in (1, 2, 4):
            pl.semaphore_signal(barrier, 1, device_id={"dp": flip(d, bit)}, device_id_type=MESH)
        count = 3

    @pl.when(z > 0)
    def _():
        pl.semaphore_signal(barrier, 1, device_id={"sp": z - 1}, device_id_type=MESH)

    @pl.when(z < last)
    def _():
        pl.semaphore_signal(barrier, 1, device_id={"sp": z + 1}, device_id_type=MESH)

    count = count + jnp.where(z > 0, 1, 0) + jnp.where(z < last, 1, 0)
    pl.semaphore_wait(barrier, count)

    if gather:
        w_all, own_sem, w_send, w_recv = w_scratch
        core, xp, yp = flip(d, 1), flip(d, 2), flip(d, 4)
        diag = flip(xp, 4)
        core_x, core_y, core_diag = flip(xp, 1), flip(yp, 1), flip(diag, 1)
        deep = w_ref.shape[0] // PIECES
        half = PIECES // 2
        x_order = list(range(PIECES))
        y_order = x_order[half:] + x_order[:half]

        def part(piece):
            return pl.ds(piece * deep, deep)

        def copy_of(lane, piece, block, target, source=None):
            rows = part(piece)
            src = w_all.at[block, rows] if source is None else source.at[rows]
            return pltpu.make_async_remote_copy(
                src_ref=src,
                dst_ref=w_all.at[block, rows],
                send_sem=w_send.at[lane, piece],
                recv_sem=w_recv.at[lane, piece],
                device_id={"dp": target},
                device_id_type=MESH,
            )

        for x_piece, y_piece in zip(x_order, y_order):
            copy_of(0, x_piece, d, xp, w_ref).start()
            copy_of(1, y_piece, d, yp, w_ref).start()
        for piece in range(PIECES):
            copy_of(3, piece, d, core, w_ref).start()
        own = pltpu.make_async_copy(w_ref, w_all.at[d], own_sem)
        own.start()

        def pass_on(step):
            piece = x_order[step]
            copy_of(0, piece, xp, xp).wait_recv()
            copy_of(4, piece, xp, core).start()
            if step < half:
                copy_of(2, piece, xp, yp).start()
            piece = y_order[step]
            copy_of(1, piece, yp, yp).wait_recv()
            copy_of(5, piece, yp, core).start()
            if step < half:
                copy_of(2, piece, yp, xp).start()

    forget = forget_ref[0].astype(F32)
    gain = in_ref[0].astype(F32)
    decay = -(jnp.log1p(jnp.exp(-jnp.abs(forget))) + jnp.maximum(-forget, 0.0))
    row_id = lax.broadcasted_iota(jnp.int32, (tokens, tokens), 0)
    col_id = lax.broadcasted_iota(jnp.int32, (tokens, tokens), 1)
    running = jnp.dot(
        decay, (row_id <= col_id).astype(F32), precision=HIGHEST, preferred_element_type=F32
    )
    offset = gain - running
    end = running[:, tokens - 1 : tokens]
    top_here = end + jnp.max(offset, axis=1, keepdims=True)
    weight = jnp.exp(end + offset - top_here)
    rows_ref[...] = jnp.zeros_like(rows_ref)
    rows_ref[0:heads] = running
    rows_ref[heads : 2 * heads] = weight * scale
    cols_ref[...] = rows_ref[...].T

    for h in range(heads):
        keys = k_ref[0, :, h * dk : (h + 1) * dk].astype(F32)
        weighted = keys * cols_ref[:, heads + h : heads + h + 1]
        kw_ref[:, h * dk : (h + 1) * dk] = weighted.astype(BF16)
        nloc_ref[h : h + 1] = jnp.sum(weighted, axis=0, keepdims=True)

    def own_state(h):
        kv_ref[h] = lax.dot_general(
            kw_ref[:, h * dk : (h + 1) * dk],
            v_ref[0, :, h * dv : (h + 1) * dv],
            (((0,), (0,)), ((), ())),
            preferred_element_type=F32,
        )

    def aux_copy():
        return pltpu.make_async_remote_copy(
            src_ref=aux_out, dst_ref=aux_in, send_sem=aux_sem.at[0], recv_sem=aux_sem.at[1],
            device_id={"sp": jnp.minimum(z + 1, last)}, device_id_type=MESH,
        )

    def state_copy(j):
        return pltpu.make_async_remote_copy(
            src_ref=state_out.at[j], dst_ref=state_in.at[j],
            send_sem=state_send.at[j], recv_sem=state_recv.at[j],
            device_id={"sp": jnp.minimum(z + 1, last)}, device_id_type=MESH,
        )

    def aux_step(m, normer):
        top = jnp.maximum(end + m, top_here)
        keep = jnp.exp(end + m - top)
        add = jnp.exp(top_here - top)
        aux_out[0:heads] = keep * normer + add * nloc_ref[...]
        aux_out[heads : 2 * heads] = jnp.broadcast_to(top, (heads, dk))
        return keep, add

    def chunk_of(j):
        h, c = j // per_head, j % per_head
        return h, slice(c * wide, (c + 1) * wide), slice(h * dv + c * wide, h * dv + (c + 1) * wide)

    @pl.when(z == 0)
    def _():
        zero = jnp.zeros((heads, 1), F32)
        _, add = aux_step(zero, jnp.zeros((heads, dk), F32))
        aux_copy().start()
        for h in range(heads):
            own_state(h)
            for c in range(per_head):
                j = h * per_head + c
                _, inner, _ = chunk_of(j)
                state_out[j] = (add[h : h + 1] * kv_ref[h, :, inner]).astype(state_out.dtype)
                state_copy(j).start()
        aux_in[...] = jnp.zeros_like(aux_in)
        state_in[...] = jnp.zeros_like(state_in)

    @pl.when((z > 0) & (z < last))
    def _():
        for h in range(heads):
            own_state(h)

    tops, dens = [], []
    for h in range(heads):
        query = q_ref[0, :, h * dk : (h + 1) * dk]
        raw = lax.dot_general(
            query, k_ref[0, :, h * dk : (h + 1) * dk], (((1,), (1,)), ((), ())),
            preferred_element_type=F32,
        )
        log_weight = cols_ref[:, h : h + 1] + offset[h : h + 1]
        log_weight = jnp.where(row_id >= col_id, log_weight, -jnp.inf)
        top = jnp.max(log_weight, axis=1, keepdims=True)
        scores = (raw * scale) * jnp.exp(log_weight - top)
        tops.append(top)
        dens.append(jnp.sum(scores, axis=1, keepdims=True))
        high = scores.astype(BF16)
        low = (scores - high.astype(F32)).astype(BF16)
        value = v_ref[0, :, h * dv : (h + 1) * dv]
        num_ref[:, h * dv : (h + 1) * dv] = jnp.dot(
            high, value, preferred_element_type=F32
        ) + jnp.dot(low, value, preferred_element_type=F32)

    @pl.when(z > 0)
    def _():
        aux_copy().wait_recv()

    m = aux_in[heads : 2 * heads, 0:1]

    @pl.when((z > 0) & (z < last))
    def _():
        aux_step(m, aux_in[0:heads])
        aux_copy().start()

    top_next = jnp.maximum(end + m, top_here)
    keep = jnp.exp(end + m - top_next)
    add = jnp.exp(top_here - top_next)

    for j in range(total):
        h, inner, outer = chunk_of(j)
        if gather:
            for step in range(PIECES):
                place = [min(max(2 * step + 2 - 3 * s, 0), total - 1) for s in range(n_sp)]
                hits = [s for s in range(n_sp) if place[s] == j]
                if hits:

                    @pl.when((z >= hits[0]) & (z <= hits[-1]))
                    def _(step=step):
                        pass_on(step)

        @pl.when(z > 0)
        def _():
            state_copy(j).wait_recv()

        @pl.when((z > 0) & (z < last))
        def _():
            state_out[j] = (
                keep[h : h + 1] * state_in[j].astype(F32) + add[h : h + 1] * kv_ref[h, :, inner]
            ).astype(state_out.dtype)
            state_copy(j).start()

        query = q_ref[0, :, h * dk : (h + 1) * dk]
        if j % per_head == 0:
            carried = cols_ref[:, h : h + 1] + m[h : h + 1]
            top = jnp.maximum(carried, tops[h])
            local = jnp.exp(tops[h] - top)
            past = jnp.exp(carried - top)
            den = local * dens[h] + past * jnp.sum(
                query.astype(F32) * aux_in[h : h + 1], axis=1, keepdims=True
            )
            inverse = 1.0 / jnp.maximum(jnp.abs(den), 1.0)
            local, past = local * inverse, past * inverse
        cell = local * num_ref[:, outer] + past * split_dot(query, state_in[j])
        hidden = cell.astype(BF16).astype(F32)
        gate = jax.nn.sigmoid(gate_ref[0, :, outer].astype(F32))
        gated_ref[:, outer] = (hidden * gate).astype(BF16)

    if not gather:
        o_ref[0] = jnp.dot(gated_ref[...], w_ref[...], preferred_element_type=F32).astype(BF16)
    else:
        cols = w_ref.shape[1]

        def column(block):
            return pl.ds(pl.multiple_of(block * cols, cols), cols)

        def project(block):
            o_ref[0, :, column(block)] = jnp.dot(
                gated_ref[...], w_all[block], preferred_element_type=F32
            ).astype(BF16)

        own.wait()
        project(d)
        for piece in range(PIECES):
            copy_of(3, piece, core, core).wait_recv()
        project(core)
        project(xp)
        project(yp)
        for piece in range(PIECES):
            copy_of(4, piece, core_x, core).wait_recv()
        project(core_x)
        for piece in range(PIECES):
            copy_of(5, piece, core_y, core).wait_recv()
        project(core_y)
        mine = jnp.zeros((tokens, cols), F32)
        other = jnp.zeros((tokens, cols), F32)
        order = [p for pair in zip(x_order[:half], y_order[:half]) for p in pair]
        for piece in order:
            copy_of(2, piece, diag, yp).wait_recv()
            copy_of(6, piece, diag, core).start()
            rows = slice(piece * deep, (piece + 1) * deep)
            mine += jnp.dot(gated_ref[:, rows], w_all[diag, rows], preferred_element_type=F32)
        o_ref[0, :, column(diag)] = mine.astype(BF16)
        for piece in order:
            copy_of(6, piece, core_diag, core).wait_recv()
            rows = slice(piece * deep, (piece + 1) * deep)
            other += jnp.dot(gated_ref[:, rows], w_all[core_diag, rows], preferred_element_type=F32)
        o_ref[0, :, column(core_diag)] = other.astype(BF16)
        for piece in range(PIECES):
            copy_of(0, piece, d, xp, w_ref).wait_send()
            copy_of(1, piece, d, yp, w_ref).wait_send()
            copy_of(3, piece, d, core, w_ref).wait_send()
            copy_of(4, piece, xp, core).wait_send()
            copy_of(5, piece, yp, core).wait_send()
            copy_of(6, piece, diag, core).wait_send()
            copy_of(2, piece, xp if piece < half else yp, core).wait_send()

    @pl.when(z < last)
    def _():
        aux_copy().wait_send()
        for j in range(total):
            state_copy(j).wait_send()


def body(n_sp, n_dp, queries, key_rows, values, out_gate, input_gate, forget_gate, out_weight):
    heads = input_gate.shape[1]
    tokens = queries.shape[1]
    dk = queries.shape[2] // heads
    width = values.shape[2]
    dv = width // heads
    wide = min(128, dv)
    total = heads * (dv // wide)
    state_type = BF16 if n_sp <= 4 else F32
    depth, cols = out_weight.shape
    gather = n_dp == 8 and cols % 128 == 0
    scratch = [
        pltpu.VMEM((tokens, tokens), F32),
        pltpu.VMEM((tokens, tokens), F32),
        pltpu.VMEM((tokens, heads * dk), BF16),
        pltpu.VMEM((heads, dk), F32),
        pltpu.VMEM((heads, dk, dv), F32),
        pltpu.VMEM((tokens, width), F32),
        pltpu.VMEM((tokens, width), BF16),
        pltpu.VMEM((2 * heads, dk), F32),
        pltpu.VMEM((2 * heads, dk), F32),
        pltpu.VMEM((total, dk, wide), state_type),
        pltpu.VMEM((total, dk, wide), state_type),
        pltpu.SemaphoreType.DMA((2,)),
        pltpu.SemaphoreType.DMA((total,)),
        pltpu.SemaphoreType.DMA((total,)),
    ]
    vmem = pl.BlockSpec(memory_space=pltpu.VMEM)
    w_spec = vmem
    if gather:
        scratch += [
            pltpu.VMEM((n_dp, depth, cols), BF16),
            pltpu.SemaphoreType.DMA,
            pltpu.SemaphoreType.DMA((7, PIECES)),
            pltpu.SemaphoreType.DMA((7, PIECES)),
        ]
        w_spec = pl.BlockSpec(memory_space=pl.ANY)
    else:
        out_weight = lax.all_gather(out_weight, "dp", axis=1, tiled=True)
    out_width = cols * n_dp
    return pl.pallas_call(
        functools.partial(kernel, n_sp, n_dp, heads, gather),
        out_shape=jax.ShapeDtypeStruct((1, tokens, out_width), BF16),
        in_specs=[vmem] * 6 + [w_spec],
        out_specs=vmem,
        scratch_shapes=scratch,
        compiler_params=pltpu.CompilerParams(
            collective_id=0, has_side_effects=True, vmem_limit_bytes=56 * 1024 * 1024
        ),
    )(queries, key_rows, values, out_gate, input_gate, forget_gate, out_weight)


def solution(mesh):
    n_sp, n_dp = mesh.shape["sp"], mesh.shape["dp"]
    return jax.shard_map(
        functools.partial(body, n_sp, n_dp),
        mesh=mesh,
        in_specs=(
            P("dp", "sp", None),
            P("dp", "sp", None),
            P("dp", "sp", None),
            P("dp", "sp", None),
            P("dp", None, "sp"),
            P("dp", None, "sp"),
            P(None, "dp"),
        ),
        out_specs=P("dp", "sp", None),
        check_vma=False,
    )
```

time: 122 us -> 47.3 us (0.39)
  the two profiles are of different devices: /device:TPU:0 before, /device:TPU:25 now
where the time goes in v1:
time: 47.3 us; the launch traced here: 47.1 us
  Pallas kernels  45.2 us (96%)
  local copies, waits for them, and re-layouts  1.88 us (4%)
    pallas_call x1, Pallas kernels, body(): pl.pallas_call(functools.partial(kernel, n_sp, n_dp, heads, gather), out_...  45.2 us
    unnamed x1, local copies, waits for them, and re-layouts  1.88 us

profile of v1, /device:TPU:25, one launch (start us, length us, event | category | flops | bytes accessed | tf_op | source)
XLA Modules:
  0.0 47.1 jit_solution(11540984765374418623)
XLA Ops:
  0.0 45.2 %shard_map.73 = bf16[1,128,2048]{2,1,0:T(8,128)(2,1)} custom-call(bf16[1,128,1024]{2,1,0:T(8,128)(2,1)} %q_ref.1, bf16[1,128,1024]{2,1,0:T(8,128)(2,1)} %k_ref.1, bf16[1,128,2048]{2,1,0:T(8,128)(2,1)} %v_ref.1, bf16[1,128,2048]{2,1,0:T(8,128)(2,1)} %gate_ref.1, bf16[1,4,128]{2,1,0:T(4,128)(2,1)} %in_ref.1, bf16[1,4,128]{2,1,0:T(4,128)(2,1)} %forget_ref.1, ...), custom_call_target="tpu_custom_call" | custom-call | tf_op jit(solution)/shard_map/pallas_call | solution.py:358
  45.2 1.9 %copy.9 = bf16[1,128,2048]{2,1,0:T(8,128)(2,1)} copy(bf16[1,128,2048]{2,1,0:T(8,128)(2,1)} %shard_map.73) | data formatting | bytes 1048576

commit v2 on v1

--- a/solution.py
+++ b/solution.py
@@ -11,6 +11,7 @@
 BF16 = jnp.bfloat16
 MESH = pl.DeviceIdType.MESH
 PIECES = 8
+SHARE = 2
 HIGHEST = lax.Precision.HIGHEST
 
 
@@ -30,7 +31,9 @@
 
 def kernel(
     n_sp, n_dp, heads, gather,
-    q_ref, k_ref, v_ref, gate_ref, in_ref, forget_ref, w_ref, o_ref,
+    q_hbm, k_hbm, v_hbm, gate_hbm, in_hbm, forget_hbm, w_ref, o_ref,
+    q_ref, k_ref, v_ref, gate_ref, in_ref, forget_ref, load_sem,
+    q_next, prod_in, prod_out, q_sem,
     rows_ref, cols_ref, kw_ref, nloc_ref, kv_ref, num_ref, gated_ref,
     aux_in, aux_out, state_in, state_out, aux_sem, state_send, state_recv,
     *w_scratch,
@@ -45,8 +48,31 @@
     per_head = total // heads
     wide = state_in.shape[2]
     last = n_sp - 1
+    relay = n_sp > 2 and tokens < dk
+
+    def q_copy(target):
+        return pltpu.make_async_remote_copy(
+            src_ref=q_ref.at[0], dst_ref=q_next, send_sem=q_sem.at[0], recv_sem=q_sem.at[1],
+            device_id={"sp": target}, device_id_type=MESH,
+        )
+
 
     barrier = pltpu.get_barrier_semaphore()
+    loads = [
+        pltpu.make_async_copy(source, target, load_sem.at[n])
+        for n, (source, target) in enumerate(
+            (
+                (in_hbm, in_ref),
+                (forget_hbm, forget_ref),
+                (k_hbm, k_ref),
+                (v_hbm, v_ref),
+                (q_hbm, q_ref),
+                (gate_hbm, gate_ref),
+            )
+        )
+    ]
+    for load in loads:
+        load.start()
     count = 0
     if gather:
         for bit in (1, 2, 4):
@@ -71,13 +97,20 @@
         core_x, core_y, core_diag = flip(xp, 1), flip(yp, 1), flip(diag, 1)
         deep = w_ref.shape[0] // PIECES
         half = PIECES // 2
-        x_order = list(range(PIECES))
-        y_order = x_order[half:] + x_order[:half]
+        odd = z % 2
+        fresh = [n + SHARE * odd for n in range(SHARE)]
+        shared = [n + SHARE * (1 - odd) for n in range(SHARE)]
+        rest = list(range(2 * SHARE, PIECES))
+        cut = half - SHARE
+        x_order = fresh + rest[:cut] + rest[cut:]
+        y_order = shared + rest[cut : 2 * cut] + rest[:cut] + rest[2 * cut :]
+        to_y, to_x = x_order[:half], y_order[:half]
+        direct = PIECES - SHARE
 
         def part(piece):
-            return pl.ds(piece * deep, deep)
-
-        def copy_of(lane, piece, block, target, source=None):
+            return pl.ds(pl.multiple_of(piece * deep, deep), deep)
+
+        def copy_of(lane, piece, block, target, source=None, axis="dp"):
             rows = part(piece)
             src = w_all.at[block, rows] if source is None else source.at[rows]
             return pltpu.make_async_remote_copy(
@@ -85,11 +118,11 @@
                 dst_ref=w_all.at[block, rows],
                 send_sem=w_send.at[lane, piece],
                 recv_sem=w_recv.at[lane, piece],
-                device_id={"dp": target},
+                device_id={axis: target},
                 device_id_type=MESH,
             )
 
-        for x_piece, y_piece in zip(x_order, y_order):
+        for x_piece, y_piece in zip(x_order[:direct], y_order[:direct]):
             copy_of(0, x_piece, d, xp, w_ref).start()
             copy_of(1, y_piece, d, yp, w_ref).start()
         for piece in range(PIECES):
@@ -98,16 +131,30 @@
         own.start()
 
         def pass_on(step):
-            piece = x_order[step]
-            copy_of(0, piece, xp, xp).wait_recv()
-            copy_of(4, piece, xp, core).start()
-            if step < half:
-                copy_of(2, piece, xp, yp).start()
-            piece = y_order[step]
-            copy_of(1, piece, yp, yp).wait_recv()
-            copy_of(5, piece, yp, core).start()
-            if step < half:
-                copy_of(2, piece, yp, xp).start()
+            for lane, order, block, target in ((0, x_order, xp, yp), (1, y_order, yp, xp)):
+                piece = order[step]
+                copy_of(lane, piece, block, block).wait_recv()
+                if step < SHARE:
+
+                    @pl.when(z == last - 1)
+                    def _():
+                        copy_of(9 + lane, piece, block, last, axis="sp").start()
+
+                    @pl.when(z > 0)
+                    def _():
+                        copy_of(7 + lane, piece, block, z - 1, axis="sp").start()
+
+                if step < half:
+                    copy_of(2, piece, block, target).start()
+                copy_of(4 + lane, piece, block, core).start()
+
+    for load in loads:
+        load.wait()
+    if relay:
+
+        @pl.when(z == last)
+        def _():
+            q_copy(last - 1).start()
 
     forget = forget_ref[0].astype(F32)
     gain = in_ref[0].astype(F32)
@@ -153,6 +200,13 @@
             device_id={"sp": jnp.minimum(z + 1, last)}, device_id_type=MESH,
         )
 
+    def prod_copy(j):
+        return pltpu.make_async_remote_copy(
+            src_ref=prod_out.at[j], dst_ref=prod_in.at[j],
+            send_sem=state_send.at[j], recv_sem=state_recv.at[j],
+            device_id={"sp": jnp.minimum(z + 1, last)}, device_id_type=MESH,
+        )
+
     def aux_step(m, normer):
         top = jnp.maximum(end + m, top_here)
         keep = jnp.exp(end + m - top)
@@ -223,8 +277,8 @@
     for j in range(total):
         h, inner, outer = chunk_of(j)
         if gather:
-            for step in range(PIECES):
-                place = [min(max(2 * step + 2 - 3 * s, 0), total - 1) for s in range(n_sp)]
+            for step in range(half):
+                place = [min(max(2 * step + 2 - (5 * s) // 2, 0), total - 1) for s in range(n_sp)]
                 hits = [s for s in range(n_sp) if place[s] == j]
                 if hits:
 
@@ -232,16 +286,28 @@
                     def _(step=step):
                         pass_on(step)
 
-        @pl.when(z > 0)
+        def step_state():
+            return keep[h : h + 1] * state_in[j].astype(F32) + add[h : h + 1] * kv_ref[h, :, inner]
+
+        @pl.when((z > 0) & (z < (last if relay else n_sp)))
         def _():
             state_copy(j).wait_recv()
 
-        @pl.when((z > 0) & (z < last))
+        @pl.when((z > 0) & (z < (last - 1 if relay else last)))
         def _():
-            state_out[j] = (
-                keep[h : h + 1] * state_in[j].astype(F32) + add[h : h + 1] * kv_ref[h, :, inner]
-            ).astype(state_out.dtype)
+            state_out[j] = step_state().astype(state_out.dtype)
             state_copy(j).start()
+
+        if relay:
+
+            @pl.when(z == last - 1)
+            def _():
+                if j == 0:
+                    q_copy(last - 1).wait_recv()
+                prod_out[j] = split_dot(
+                    q_next[:, h * dk : (h + 1) * dk], step_state().astype(state_out.dtype)
+                ).astype(prod_out.dtype)
+                prod_copy(j).start()
 
         query = q_ref[0, :, h * dk : (h + 1) * dk]
         if j % per_head == 0:
@@ -254,10 +320,25 @@
             )
             inverse = 1.0 / jnp.maximum(jnp.abs(den), 1.0)
             local, past = local * inverse, past * inverse
-        cell = local * num_ref[:, outer] + past * split_dot(query, state_in[j])
-        hidden = cell.astype(BF16).astype(F32)
-        gate = jax.nn.sigmoid(gate_ref[0, :, outer].astype(F32))
-        gated_ref[:, outer] = (hidden * gate).astype(BF16)
+        def finish(product):
+            cell = local * num_ref[:, outer] + past * product
+            hidden = cell.astype(BF16).astype(F32)
+            gate = jax.nn.sigmoid(gate_ref[0, :, outer].astype(F32))
+            gated_ref[:, outer] = (hidden * gate).astype(BF16)
+
+        if relay:
+
+            @pl.when(z < last)
+            def _():
+                finish(split_dot(query, state_in[j]))
+
+            @pl.when(z == last)
+            def _():
+                prod_copy(j).wait_recv()
+                finish(prod_in[j].astype(F32))
+
+        else:
+            finish(split_dot(query, state_in[j]))
 
     if not gather:
         o_ref[0] = jnp.dot(gated_ref[...], w_ref[...], preferred_element_type=F32).astype(BF16)
@@ -272,8 +353,22 @@
                 gated_ref[...], w_all[block], preferred_element_type=F32
             ).astype(BF16)
 
+        for step in range(half, direct):
+            pass_on(step)
         own.wait()
         project(d)
+        for n in range(SHARE):
+            for lane, piece, block in ((0, shared[n], xp), (1, fresh[n], yp)):
+
+                @pl.when(z < last)
+                def _():
+                    copy_of(7 + lane, piece, block, 0, axis="sp").wait_recv()
+
+                @pl.when(z == last)
+                def _():
+                    copy_of(9 + lane, piece, block, 0, axis="sp").wait_recv()
+
+                copy_of(4 + lane, piece, block, core).start()
         for piece in range(PIECES):
             copy_of(3, piece, core, core).wait_recv()
         project(core)
@@ -287,28 +382,53 @@
         project(core_y)
         mine = jnp.zeros((tokens, cols), F32)
         other = jnp.zeros((tokens, cols), F32)
-        order = [p for pair in zip(x_order[:half], y_order[:half]) for p in pair]
+        order = [p for pair in zip(to_y, to_x) for p in pair]
         for piece in order:
             copy_of(2, piece, diag, yp).wait_recv()
             copy_of(6, piece, diag, core).start()
-            rows = slice(piece * deep, (piece + 1) * deep)
+            rows = part(piece)
             mine += jnp.dot(gated_ref[:, rows], w_all[diag, rows], preferred_element_type=F32)
         o_ref[0, :, column(diag)] = mine.astype(BF16)
         for piece in order:
             copy_of(6, piece, core_diag, core).wait_recv()
-            rows = slice(piece * deep, (piece + 1) * deep)
+            rows = part(piece)
             other += jnp.dot(gated_ref[:, rows], w_all[core_diag, rows], preferred_element_type=F32)
         o_ref[0, :, column(core_diag)] = other.astype(BF16)
         for piece in range(PIECES):
-            copy_of(0, piece, d, xp, w_ref).wait_send()
-            copy_of(1, piece, d, yp, w_ref).wait_send()
             copy_of(3, piece, d, core, w_ref).wait_send()
             copy_of(4, piece, xp, core).wait_send()
             copy_of(5, piece, yp, core).wait_send()
             copy_of(6, piece, diag, core).wait_send()
-            copy_of(2, piece, xp if piece < half else yp, core).wait_send()
-
-    @pl.when(z < last)
+        for step in range(direct):
+            copy_of(0, x_order[step], d, xp, w_ref).wait_send()
+            copy_of(1, y_order[step], d, yp, w_ref).wait_send()
+        for step in range(half):
+            copy_of(2, to_y[step], xp, yp).wait_send()
+            copy_of(2, to_x[step], yp, xp).wait_send()
+        for n in range(SHARE):
+            for lane, piece, block in ((0, fresh[n], xp), (1, shared[n], yp)):
+
+                @pl.when(z == last - 1)
+                def _():
+                    copy_of(9 + lane, piece, block, 0, axis="sp").wait_send()
+
+                @pl.when(z > 0)
+                def _():
+                    copy_of(7 + lane, piece, block, 0, axis="sp").wait_send()
+
+    if relay:
+
+        @pl.when(z == last)
+        def _():
+            q_copy(last - 1).wait_send()
+
+        @pl.when(z == last - 1)
+        def _():
+            aux_copy().wait_send()
+            for j in range(total):
+                prod_copy(j).wait_send()
+
+    @pl.when(z < (last - 1 if relay else last))
     def _():
         aux_copy().wait_send()
         for j in range(total):
@@ -326,7 +446,13 @@
     state_type = BF16 if n_sp <= 4 else F32
     depth, cols = out_weight.shape
     gather = n_dp == 8 and cols % 128 == 0
-    scratch = [
+    loaded = (queries, key_rows, values, out_gate, input_gate, forget_gate)
+    scratch = [pltpu.VMEM(source.shape, source.dtype) for source in loaded] + [
+        pltpu.SemaphoreType.DMA((len(loaded),)),
+        pltpu.VMEM((tokens, heads * dk), BF16),
+        pltpu.VMEM((total, tokens, wide), state_type),
+        pltpu.VMEM((total, tokens, wide), state_type),
+        pltpu.SemaphoreType.DMA((2,)),
         pltpu.VMEM((tokens, tokens), F32),
         pltpu.VMEM((tokens, tokens), F32),
         pltpu.VMEM((tokens, heads * dk), BF16),
@@ -348,8 +474,8 @@
         scratch += [
             pltpu.VMEM((n_dp, depth, cols), BF16),
             pltpu.SemaphoreType.DMA,
-            pltpu.SemaphoreType.DMA((7, PIECES)),
-            pltpu.SemaphoreType.DMA((7, PIECES)),
+            pltpu.SemaphoreType.DMA((11, PIECES)),
+            pltpu.SemaphoreType.DMA((11, PIECES)),
         ]
         w_spec = pl.BlockSpec(memory_space=pl.ANY)
     else:
@@ -358,7 +484,7 @@
     return pl.pallas_call(
         functools.partial(kernel, n_sp, n_dp, heads, gather),
         out_shape=jax.ShapeDtypeStruct((1, tokens, out_width), BF16),
-        in_specs=[vmem] * 6 + [w_spec],
+        in_specs=[pl.BlockSpec(memory_space=pl.ANY)] * 6 + [w_spec],
         out_specs=vmem,
         scratch_shapes=scratch,
         compiler_params=pltpu.CompilerParams(

time: 47.3 us -> 44.2 us (0.934)
  Pallas kernels: 45.2 us -> 42.1 us
    pallas_call x1, Pallas kernels: 45.2 us -> 42.1 us  [body(): pl.pallas_call(functools.partial(kernel, n_sp, n_dp, heads, gather), out_...]
where the time goes in v2:
time: 44.2 us; the launch traced here: 44 us
  Pallas kernels  42.1 us (95%)
  local copies, waits for them, and re-layouts  1.88 us (4%)
    pallas_call x1, Pallas kernels, body(): pl.pallas_call(functools.partial(kernel, n_sp, n_dp, heads, gather), out_...  42.1 us
    unnamed x1, local copies, waits for them, and re-layouts  1.88 us

profile of v2, /device:TPU:25, one launch (start us, length us, event | category | flops | bytes accessed | tf_op | source)
XLA Modules:
  0.0 44.0 jit_solution(17306651030974762063)
XLA Ops:
  0.0 42.1 %shard_map.73 = bf16[1,128,2048]{2,1,0:T(8,128)(2,1)} custom-call(bf16[1,128,1024]{2,1,0:T(8,128)(2,1)} %q_hbm.1, bf16[1,128,1024]{2,1,0:T(8,128)(2,1)} %k_hbm.1, bf16[1,128,2048]{2,1,0:T(8,128)(2,1)} %v_hbm.1, bf16[1,128,2048]{2,1,0:T(8,128)(2,1)} %gate_hbm.1, bf16[1,4,128]{2,1,0:T(4,128)(2,1)} %in_hbm.1, bf16[1,4,128]{2,1,0:T(4,128)(2,1)} %forget_hbm.1, ...), custom_call_target="tpu_custom_call" | custom-call | tf_op jit(solution)/shard_map/pallas_call | solution.py:484
  42.1 1.9 %copy.9 = bf16[1,128,2048]{2,1,0:T(8,128)(2,1)} copy(bf16[1,128,2048]{2,1,0:T(8,128)(2,1)} %shard_map.73) | data formatting | bytes 1048576

commit v3 on v2

--- a/solution.py
+++ b/solution.py
@@ -12,6 +12,7 @@
 MESH = pl.DeviceIdType.MESH
 PIECES = 8
 SHARE = 2
+VMEM_BYTES = 67_043_328
 HIGHEST = lax.Precision.HIGHEST
 
 
@@ -91,7 +92,7 @@
     pl.semaphore_wait(barrier, count)
 
     if gather:
-        w_all, own_sem, w_send, w_recv = w_scratch
+        w_all, acc_ref, own_sem, w_send, w_recv = w_scratch
         core, xp, yp = flip(d, 1), flip(d, 2), flip(d, 4)
         diag = flip(xp, 4)
         core_x, core_y, core_diag = flip(xp, 1), flip(yp, 1), flip(diag, 1)
@@ -236,11 +237,9 @@
 
     @pl.when((z > 0) & (z < last))
     def _():
-        for h in range(heads):
-            own_state(h)
-
-    tops, dens = [], []
-    for h in range(heads):
+        own_state(0)
+
+    def own_rows(h):
         query = q_ref[0, :, h * dk : (h + 1) * dk]
         raw = lax.dot_general(
             query, k_ref[0, :, h * dk : (h + 1) * dk], (((1,), (1,)), ((), ())),
@@ -250,14 +249,13 @@
         log_weight = jnp.where(row_id >= col_id, log_weight, -jnp.inf)
         top = jnp.max(log_weight, axis=1, keepdims=True)
         scores = (raw * scale) * jnp.exp(log_weight - top)
-        tops.append(top)
-        dens.append(jnp.sum(scores, axis=1, keepdims=True))
         high = scores.astype(BF16)
         low = (scores - high.astype(F32)).astype(BF16)
         value = v_ref[0, :, h * dv : (h + 1) * dv]
         num_ref[:, h * dv : (h + 1) * dv] = jnp.dot(
             high, value, preferred_element_type=F32
         ) + jnp.dot(low, value, preferred_element_type=F32)
+        return top, jnp.sum(scores, axis=1, keepdims=True)
 
     @pl.when(z > 0)
     def _():
@@ -274,8 +272,52 @@
     keep = jnp.exp(end + m - top_next)
     add = jnp.exp(top_here - top_next)
 
+    if gather:
+        cols = w_ref.shape[1]
+        width = gated_ref.shape[1]
+        early = slice(0, width - dv)
+        late = slice(width - dv, width)
+        pairs = list(zip(to_y, to_x))
+
+        def column(block):
+            return pl.ds(pl.multiple_of(block * cols, cols), cols)
+
+        def begin(block):
+            acc_ref[:, column(block)] = jnp.dot(
+                gated_ref[:, early], w_all[block, early], preferred_element_type=F32
+            )
+
+        def end_of(block):
+            o_ref[0, :, column(block)] = (
+                acc_ref[:, column(block)]
+                + jnp.dot(gated_ref[:, late], w_all[block, late], preferred_element_type=F32)
+            ).astype(BF16)
+
+        def rest_of_blocks():
+            for step in range(half, direct):
+                pass_on(step)
+            for n in range(SHARE):
+                for lane, piece, block in ((0, shared[n], xp), (1, fresh[n], yp)):
+
+                    @pl.when(z < last)
+                    def _():
+                        copy_of(7 + lane, piece, block, 0, axis="sp").wait_recv()
+
+                    @pl.when(z == last)
+                    def _():
+                        copy_of(9 + lane, piece, block, 0, axis="sp").wait_recv()
+
+                    copy_of(4 + lane, piece, block, core).start()
+
+        def diagonal(pair):
+            for piece in pair:
+                copy_of(2, piece, diag, yp).wait_recv()
+                copy_of(6, piece, diag, core).start()
+
     for j in range(total):
         h, inner, outer = chunk_of(j)
+        if gather and j == total - per_head - 2:
+            rest_of_blocks()
         if gather:
             for step in range(half):
                 place = [min(max(2 * step + 2 - (5 * s) // 2, 0), total - 1) for s in range(n_sp)]
@@ -309,13 +351,20 @@
                 ).astype(prod_out.dtype)
                 prod_copy(j).start()
 
+        if j % per_head == per_head - 1 and h + 1 < heads:
+
+            @pl.when((z > 0) & (z < last))
+            def _():
+                own_state(h + 1)
+
         query = q_ref[0, :, h * dk : (h + 1) * dk]
         if j % per_head == 0:
+            top_own, den_own = own_rows(h)
             carried = cols_ref[:, h : h + 1] + m[h : h + 1]
-            top = jnp.maximum(carried, tops[h])
-            local = jnp.exp(tops[h] - top)
+            top = jnp.maximum(carried, top_own)
+            local = jnp.exp(top_own - top)
             past = jnp.exp(carried - top)
-            den = local * dens[h] + past * jnp.sum(
+            den = local * den_own + past * jnp.sum(
                 query.astype(F32) * aux_in[h : h + 1], axis=1, keepdims=True
             )
             inverse = 1.0 / jnp.maximum(jnp.abs(den), 1.0)
@@ -340,59 +389,39 @@
         else:
             finish(split_dot(query, state_in[j]))
 
+        if gather:
+            ready = j - (total - per_head - 1)
+            if ready == 0:
+                own.wait()
+                for piece in range(PIECES):
+                    copy_of(3, piece, core, core).wait_recv()
+                begin(d)
+                begin(core)
+            elif ready == 1:
+                begin(xp)
+                begin(yp)
+            elif ready == 2:
+                for piece in range(PIECES):
+                    copy_of(4, piece, core_x, core).wait_recv()
+                    copy_of(5, piece, core_y, core).wait_recv()
+                begin(core_x)
+                begin(core_y)
+                diagonal(pairs[0])
+            elif ready == 3:
+                diagonal(pairs[1])
+
     if not gather:
         o_ref[0] = jnp.dot(gated_ref[...], w_ref[...], preferred_element_type=F32).astype(BF16)
     else:
-        cols = w_ref.shape[1]
-
-        def column(block):
-            return pl.ds(pl.multiple_of(block * cols, cols), cols)
-
-        def project(block):
-            o_ref[0, :, column(block)] = jnp.dot(
-                gated_ref[...], w_all[block], preferred_element_type=F32
-            ).astype(BF16)
-
-        for step in range(half, direct):
-            pass_on(step)
-        own.wait()
-        project(d)
-        for n in range(SHARE):
-            for lane, piece, block in ((0, shared[n], xp), (1, fresh[n], yp)):
-
-                @pl.when(z < last)
-                def _():
-                    copy_of(7 + lane, piece, block, 0, axis="sp").wait_recv()
-
-                @pl.when(z == last)
-                def _():
-                    copy_of(9 + lane, piece, block, 0, axis="sp").wait_recv()
-
-                copy_of(4 + lane, piece, block, core).start()
+        for block in (d, core, xp, yp, core_x, core_y):
+            end_of(block)
+        for pair in pairs[2:]:
+            diagonal(pair)
+        mine = jnp.dot(gated_ref[...], w_all[diag], preferred_element_type=F32)
+        o_ref[0, :, column(diag)] = mine.astype(BF16)
         for piece in range(PIECES):
-            copy_of(3, piece, core, core).wait_recv()
-        project(core)
-        project(xp)
-        project(yp)
-        for piece in range(PIECES):
-            copy_of(4, piece, core_x, core).wait_recv()
-        project(core_x)
-        for piece in range(PIECES):
-            copy_of(5, piece, core_y, core).wait_recv()
-        project(core_y)
-        mine = jnp.zeros((tokens, cols), F32)
-        other = jnp.zeros((tokens, cols), F32)
-        order = [p for pair in zip(to_y, to_x) for p in pair]
-        for piece in order:
-            copy_of(2, piece, diag, yp).wait_recv()
-            copy_of(6, piece, diag, core).start()
-            rows = part(piece)
-            mine += jnp.dot(gated_ref[:, rows], w_all[diag, rows], preferred_element_type=F32)
-        o_ref[0, :, column(diag)] = mine.astype(BF16)
-        for piece in order:
             copy_of(6, piece, core_diag, core).wait_recv()
-            rows = part(piece)
-            other += jnp.dot(gated_ref[:, rows], w_all[core_diag, rows], preferred_element_type=F32)
+        other = jnp.dot(gated_ref[...], w_all[core_diag], preferred_element_type=F32)
         o_ref[0, :, column(core_diag)] = other.astype(BF16)
         for piece in range(PIECES):
             copy_of(3, piece, d, core, w_ref).wait_send()
@@ -473,6 +502,7 @@
     if gather:
         scratch += [
             pltpu.VMEM((n_dp, depth, cols), BF16),
+            pltpu.VMEM((tokens, cols * n_dp), F32),
             pltpu.SemaphoreType.DMA,
             pltpu.SemaphoreType.DMA((11, PIECES)),
             pltpu.SemaphoreType.DMA((11, PIECES)),
@@ -483,12 +513,12 @@
     out_width = cols * n_dp
     return pl.pallas_call(
         functools.partial(kernel, n_sp, n_dp, heads, gather),
-        out_shape=jax.ShapeDtypeStruct((1, tokens, out_width), BF16),
+        out_shape=pltpu.VMEM((1, tokens, out_width), BF16),
         in_specs=[pl.BlockSpec(memory_space=pl.ANY)] * 6 + [w_spec],
         out_specs=vmem,
         scratch_shapes=scratch,
         compiler_params=pltpu.CompilerParams(
-            collective_id=0, has_side_effects=True, vmem_limit_bytes=56 * 1024 * 1024
+            collective_id=0, has_side_effects=True, vmem_limit_bytes=VMEM_BYTES - 2 * tokens * out_width
         ),
     )(queries, key_rows, values, out_gate, input_gate, forget_gate, out_weight)
 

time: 44.2 us -> 39.4 us (0.89)
  Pallas kernels: 42.1 us -> 38.5 us
  local copies, waits for them, and re-layouts: 1.88 us -> 0.8 us
    pallas_call x1, Pallas kernels: 42.1 us -> 38.5 us  [body(): pl.pallas_call(functools.partial(kernel, n_sp, n_dp, heads, gather), out_...]
    unnamed x1, local copies, waits for them, and re-layouts: 1.88 us -> 0.8 us
where the time goes in v3:
time: 39.4 us; the launch traced here: 39.3 us
  Pallas kernels  38.5 us (98%)
  local copies, waits for them, and re-layouts  0.8 us (2%)
    pallas_call x1, Pallas kernels, body(): pl.pallas_call(functools.partial(kernel, n_sp, n_dp, heads, gather), out_...  38.5 us
    unnamed x1, local copies, waits for them, and re-layouts  0.8 us

profile of v3, /device:TPU:25, one launch (start us, length us, event | category | flops | bytes accessed | tf_op | source)
XLA Modules:
  0.0 39.3 jit_solution(11527410764677182100)
XLA Ops:
  0.0 38.5 %shard_map.73 = bf16[1,128,2048]{2,1,0:T(8,128)(2,1)S(1)} custom-call(bf16[1,128,1024]{2,1,0:T(8,128)(2,1)} %q_hbm.1, bf16[1,128,1024]{2,1,0:T(8,128)(2,1)} %k_hbm.1, bf16[1,128,2048]{2,1,0:T(8,128)(2,1)} %v_hbm.1, bf16[1,128,2048]{2,1,0:T(8,128)(2,1)} %gate_hbm.1, bf16[1,4,128]{2,1,0:T(4,128)(2,1)} %in_hbm.1, bf16[1,4,128]{2,1,0:T(4,128)(2,1)} %forget_hbm.1, ...), custom_call_target="tpu_custom_call" | custom-call | tf_op jit(solution)/shard_map/pallas_call | solution.py:514
  38.5 0.8 %copy.9 = bf16[1,128,2048]{2,1,0:T(8,128)(2,1)} copy(bf16[1,128,2048]{2,1,0:T(8,128)(2,1)S(1)} %shard_map.73) | data formatting | bytes 1048576

commit v4 on v3

--- a/solution.py
+++ b/solution.py
@@ -276,7 +276,8 @@
         cols = w_ref.shape[1]
         width = gated_ref.shape[1]
         early = slice(0, width - dv)
-        late = slice(width - dv, width)
+        middle = slice(width - dv, width - wide)
+        blocks = (d, core, xp, yp, core_x, core_y)
         pairs = list(zip(to_y, to_x))
 
         def column(block):
@@ -287,7 +288,12 @@
                 gated_ref[:, early], w_all[block, early], preferred_element_type=F32
             )
 
-        def end_of(block):
+        def more(block):
+            acc_ref[:, column(block)] += jnp.dot(
+                gated_ref[:, middle], w_all[block, middle], preferred_element_type=F32
+            )
+
+        def end_of(block, late):
             o_ref[0, :, column(block)] = (
                 acc_ref[:, column(block)]
                 + jnp.dot(gated_ref[:, late], w_all[block, late], preferred_element_type=F32)
@@ -320,7 +326,7 @@
             rest_of_blocks()
         if gather:
             for step in range(half):
-                place = [min(max(2 * step + 2 - (5 * s) // 2, 0), total - 1) for s in range(n_sp)]
+                place = [min(max(2 * step + 4 - (5 * s) // 2, 0), total - 1) for s in range(n_sp)]
                 hits = [s for s in range(n_sp) if place[s] == j]
                 if hits:
 
@@ -410,11 +416,24 @@
             elif ready == 3:
                 diagonal(pairs[1])
 
+                @pl.when(z == last)
+                def _():
+                    for block in blocks:
+                        more(block)
+
     if not gather:
         o_ref[0] = jnp.dot(gated_ref[...], w_ref[...], preferred_element_type=F32).astype(BF16)
     else:
-        for block in (d, core, xp, yp, core_x, core_y):
-            end_of(block)
+        @pl.when(z == last)
+        def _():
+            for block in blocks:
+                end_of(block, slice(width - wide, width))
+
+        @pl.when(z < last)
+        def _():
+            for block in blocks:
+                end_of(block, slice(width - dv, width))
+
         for pair in pairs[2:]:
             diagonal(pair)
         mine = jnp.dot(gated_ref[...], w_all[diag], preferred_element_type=F32)

time: 39.4 us -> 38.6 us (0.980)
  Pallas kernels: 38.5 us -> 37.7 us
    pallas_call x1, Pallas kernels: 38.5 us -> 37.7 us  [body(): pl.pallas_call(functools.partial(kernel, n_sp, n_dp, heads, gather), out_...]
where the time goes in v4:
time: 38.6 us; the launch traced here: 38.5 us
  Pallas kernels  37.7 us (98%)
  local copies, waits for them, and re-layouts  0.8 us (2%)
    pallas_call x1, Pallas kernels, body(): pl.pallas_call(functools.partial(kernel, n_sp, n_dp, heads, gather), out_...  37.7 us
    unnamed x1, local copies, waits for them, and re-layouts  0.8 us

profile of v4, /device:TPU:25, one launch (start us, length us, event | category | flops | bytes accessed | tf_op | source)
XLA Modules:
  0.0 38.5 jit_solution(14116065784030284080)
XLA Ops:
  0.0 37.7 %shard_map.73 = bf16[1,128,2048]{2,1,0:T(8,128)(2,1)S(1)} custom-call(bf16[1,128,1024]{2,1,0:T(8,128)(2,1)} %q_hbm.1, bf16[1,128,1024]{2,1,0:T(8,128)(2,1)} %k_hbm.1, bf16[1,128,2048]{2,1,0:T(8,128)(2,1)} %v_hbm.1, bf16[1,128,2048]{2,1,0:T(8,128)(2,1)} %gate_hbm.1, bf16[1,4,128]{2,1,0:T(4,128)(2,1)} %in_hbm.1, bf16[1,4,128]{2,1,0:T(4,128)(2,1)} %forget_hbm.1, ...), custom_call_target="tpu_custom_call" | custom-call | tf_op jit(solution)/shard_map/pallas_call | solution.py:533
  37.7 0.8 %copy.9 = bf16[1,128,2048]{2,1,0:T(8,128)(2,1)} copy(bf16[1,128,2048]{2,1,0:T(8,128)(2,1)S(1)} %shard_map.73) | data formatting | bytes 1048576
